TPU v7x, 32 devices: a whole 2x2x4 slice. The times are simulated.
32 devices in a mesh: sp: 8 (over z, x), tp: 4 (over y, core).
Axes of the slice: x: 2, y: 2, z: 4, core: 2. Of those that a mesh axis runs over, the one named last changes fastest.
Arguments:
- resid: bfloat16 [2048, 2048], P('sp'), may hold values from -6 to 6
- query_one: bfloat16 [2048, 1024], P('sp', 'tp'), may hold values from -400 to 400
- query_two: bfloat16 [2048, 1024], P('sp', 'tp'), may hold values from -400 to 400
- key_one: bfloat16 [2048, 1024], P('sp', 'tp'), may hold values from -8 to 8
- key_two: bfloat16 [2048, 1024], P('sp', 'tp'), may hold values from -8 to 8
- values: bfloat16 [2048, 2048], P('sp', 'tp'), may hold values from -6 to 6
- documents: int32 [2048], P('sp'), may hold values from 0 to 1, never falling along the last dimension, each value on 1 to 1280 neighbouring positions
- mix_lambda: float32 [16], P('tp'), may hold values from 0.3 to 0.8
- head_gain: float32 [128], replicated, may hold values from 0.1 to 1.9
- out_weight: bfloat16 [2048, 2048], P('tp'), may hold values from -0.125 to 0.125
- ffn_gain: float32 [2048], replicated, may hold values from 0.1 to 1.9
- routes: int32 [2048, 4], P('sp'), may hold values from 0 to 31, all different within a row; in each aligned block of 256 rows (0 to 255, 256 to 511, ...) at most 64 rows name the same one
- route_weight: float32 [2048, 4], P('sp'), may hold values from 0.2 to 0.9
- expert_gate: bfloat16 [32, 2048, 512], P(('sp', 'tp')), may hold values from -0.125 to 0.125
- expert_up: bfloat16 [32, 2048, 512], P(('sp', 'tp')), may hold values from -0.125 to 0.125
- expert_down: bfloat16 [32, 512, 2048], P(('sp', 'tp')), may hold values from -0.25 to 0.25
- shared_gate: bfloat16 [2048, 512], P(None, 'tp'), may hold values from -0.125 to 0.125
- shared_up: bfloat16 [2048, 512], P(None, 'tp'), may hold values from -0.125 to 0.125
- shared_down: bfloat16 [512, 2048], P('tp'), may hold values from -0.25 to 0.25
Outputs:
- layer_out: bfloat16 [2048, 2048], P(('sp', 'tp'))
Inputs may be any that keep to these rules, and one draw needn't show every extreme that they name: `documents`: document numbers never fall along the positions; each document has 1 to 1280 positions and one has exactly 1280. `routes`: A row names 4 different experts. In each aligned block of 256 rows no expert is named by more than 64 rows, a bound that some block reaches.
All inputs are finite; a program needn't handle non-finite values.
Results may differ from a plain program's by a relative error of at most 0.018.
Values may be sent and summed in bfloat16 or wider, within the bound.
A program may use at most 128 MiB of HBM per device.

v0:
```python
import jax
import jax.numpy as jnp
from jax import lax
from jax.sharding import PartitionSpec as P

NEG_FILL = -1e30
HEAD_SCALE = 0.8


def rms_scale(values_in, eps_value):
    return lax.rsqrt(jnp.mean(values_in * values_in, axis=-1, keepdims=True) + eps_value)


def local(
    resid,
    query_one,
    query_two,
    key_one,
    key_two,
    values,
    documents,
    mix_lambda,
    head_gain,
    out_weight,
    ffn_gain,
    routes,
    route_weight,
    expert_gate,
    expert_up,
    expert_down,
    shared_gate,
    shared_up,
    shared_down,
):
    tok_rows = query_one.shape[0]
    head_count = mix_lambda.shape[0]
    head_width = query_one.shape[1] // head_count
    value_width = values.shape[1] // head_count
    model_width = resid.shape[1]
    score_scale = head_width ** (-0.5)
    seq_size = lax.axis_size("sp")
    tp_size = lax.axis_size("tp")
    query_pos = lax.axis_index("sp") * tok_rows + jnp.arange(tok_rows, dtype=jnp.int32)
    query_first = query_one.reshape(tok_rows, head_count, head_width)
    query_second = query_two.reshape(tok_rows, head_count, head_width)
    lambda_col = mix_lambda[:, None, None]
    first_doc = documents[0]
    last_pos = query_pos[tok_rows - 1]

    def masks(key_docs):
        key_pos = jnp.arange(key_docs.shape[0], dtype=jnp.int32)
        return (
            (key_pos[None, :] <= query_pos[:, None]) & (key_docs[None, :] == documents[:, None])
        )[None]

    def needed(key_docs, offset):
        return (offset <= last_pos) & (jnp.max(key_docs) >= first_doc)

    def scores(query_block, key_block):
        keyed = key_block.reshape(key_block.shape[0], head_count, head_width)
        return (
            jnp.einsum("qhd,khd->hqk", query_block, keyed, preferred_element_type=jnp.float32)
            * score_scale
        )

    empty_max = jnp.full((head_count, tok_rows), NEG_FILL, jnp.float32)
    empty_sum = jnp.zeros((head_count, tok_rows), jnp.float32)
    stats_init = ((empty_max, empty_sum), (empty_max, empty_sum))
    value_init = jnp.zeros((head_count, tok_rows, value_width), jnp.float32)
    key_first = lax.all_gather(key_one, "sp", axis=0, tiled=True)
    key_second = lax.all_gather(key_two, "sp", axis=0, tiled=True)
    key_docs = lax.all_gather(documents, "sp", axis=0, tiled=True)

    def stats_update(current):
        allowed = masks(key_docs)
        result = []
        for query_block, key_block, (top_now, sum_now) in (
            (query_first, key_first, current[0]),
            (query_second, key_second, current[1]),
        ):
            masked = jnp.where(allowed, scores(query_block, key_block), NEG_FILL)
            top_next = jnp.maximum(top_now, jnp.max(masked, axis=-1))
            fresh = jnp.where(allowed, jnp.exp(masked - top_next[:, :, None]), 0.0)
            result.append((top_next, jnp.sum(fresh, axis=-1)))
        return tuple(result)

    def stats_keep(current):
        return current

    soft_stats = lax.cond(needed(key_docs, jnp.int32(0)), stats_update, stats_keep, stats_init)
    apply_key_first = lax.all_gather(key_one, "sp", axis=0, tiled=True)
    apply_key_second = lax.all_gather(key_two, "sp", axis=0, tiled=True)
    value_block = lax.all_gather(values, "sp", axis=0, tiled=True)
    apply_key_docs = lax.all_gather(documents, "sp", axis=0, tiled=True)

    def apply_update(current):
        allowed = masks(apply_key_docs)
        probs = []
        for query_block, key_block, (top_all, sum_all) in (
            (query_first, apply_key_first, soft_stats[0]),
            (query_second, apply_key_second, soft_stats[1]),
        ):
            raw = scores(query_block, key_block)
            probs.append(
                jnp.where(allowed, jnp.exp(raw - top_all[:, :, None]), 0.0) / sum_all[:, :, None]
            )
        weights = (probs[0] - lambda_col * probs[1]).astype(jnp.bfloat16)
        valued = value_block.reshape(value_block.shape[0], head_count, value_width)
        return current + jnp.einsum(
            "hqk,khv->hqv", weights, valued, preferred_element_type=jnp.float32
        )

    def apply_keep(current):
        return current

    head_out = lax.cond(needed(apply_key_docs, jnp.int32(0)), apply_update, apply_keep, value_init)
    normed_heads = (head_out * rms_scale(head_out, 1e-05) * head_gain * HEAD_SCALE).astype(
        jnp.bfloat16
    )
    attn_rows = normed_heads.transpose(1, 0, 2).reshape(tok_rows, head_count * value_width)
    share_rows = tok_rows // tp_size
    own_start = lax.axis_index("tp") * share_rows
    proj_term = jnp.dot(attn_rows, out_weight, preferred_element_type=jnp.float32)
    projected = lax.psum(proj_term.astype(jnp.bfloat16), "tp").astype(jnp.float32)
    mixed_all = resid.astype(jnp.float32) + projected
    normed_all = (mixed_all * rms_scale(mixed_all, 1e-06) * ffn_gain).astype(jnp.bfloat16)
    mixed_own = lax.dynamic_slice_in_dim(mixed_all, own_start, share_rows, 0)
    route_slots = routes.shape[1]
    capacity = max(2, 2 * tok_rows * route_slots // (seq_size * tp_size))
    assign_total = tok_rows * route_slots
    flat_expert = routes.reshape(assign_total)
    flat_weight = route_weight.reshape(assign_total)
    assign_token = jnp.arange(assign_total, dtype=jnp.int32) // route_slots
    is_mine = flat_expert % tp_size == lax.axis_index("tp")
    target = flat_expert // tp_size
    one_hot = (
        (target[:, None] == jnp.arange(seq_size, dtype=jnp.int32)[None, :]) & is_mine[:, None]
    ).astype(jnp.int32)
    slot_rank = jnp.sum(jnp.cumsum(one_hot, axis=0) * one_hot, axis=1) - 1
    slot_id = jnp.where(is_mine, target * capacity + slot_rank, -1)
    slot_total = seq_size * capacity
    matches = slot_id[None, :] == jnp.arange(slot_total, dtype=jnp.int32)[:, None]
    slot_token = jnp.sum(jnp.where(matches, assign_token[None, :], 0), axis=1)
    slot_live = jnp.any(matches, axis=1)
    outgoing = jnp.where(
        slot_live[:, None], normed_all[slot_token], jnp.zeros((), jnp.bfloat16)
    ).reshape(seq_size, capacity, model_width)
    arrived = lax.all_to_all(outgoing, "sp", split_axis=0, concat_axis=0, tiled=True)
    item_count = arrived.shape[1]
    flat_rows = arrived.reshape(seq_size * item_count, model_width)
    gate_part = jnp.dot(flat_rows, expert_gate[0], preferred_element_type=jnp.float32)
    up_part = jnp.dot(flat_rows, expert_up[0], preferred_element_type=jnp.float32)
    hidden = (jax.nn.silu(gate_part) * up_part).astype(jnp.bfloat16)
    result = jnp.dot(hidden, expert_down[0], preferred_element_type=jnp.float32).astype(
        jnp.bfloat16
    )
    returned = lax.all_to_all(
        result.reshape(seq_size, item_count, model_width),
        "sp",
        split_axis=0,
        concat_axis=0,
        tiled=True,
    )
    returned_flat = returned.reshape(slot_total, model_width)
    picked = returned_flat[jnp.maximum(slot_id, 0)].astype(jnp.float32)
    picked_weight = jnp.where(is_mine, flat_weight, 0.0)
    routed = jnp.sum(
        (picked * picked_weight[:, None]).reshape(tok_rows, route_slots, model_width), axis=1
    )
    shared_act = (
        jax.nn.silu(jnp.dot(normed_all, shared_gate, preferred_element_type=jnp.float32))
        * jnp.dot(normed_all, shared_up, preferred_element_type=jnp.float32)
    ).astype(jnp.bfloat16)
    shared_out = jnp.dot(shared_act, shared_down, preferred_element_type=jnp.float32)
    ffn_own = lax.psum_scatter(
        (routed + shared_out).astype(jnp.bfloat16), "tp", scatter_dimension=0, tiled=True
    ).astype(jnp.float32)
    return (mixed_own + ffn_own).astype(jnp.bfloat16)


def solution(mesh):
    placed = (
        P("sp", None),
        P("sp", "tp"),
        P("sp", "tp"),
        P("sp", "tp"),
        P("sp", "tp"),
        P("sp", "tp"),
        P("sp"),
        P("tp"),
        P(),
        P("tp", None),
        P(),
        P("sp", None),
        P("sp", None),
        P(("sp", "tp"), None, None),
        P(("sp", "tp"), None, None),
        P(("sp", "tp"), None, None),
        P(None, "tp"),
        P(None, "tp"),
        P("tp", None),
    )
    return jax.shard_map(
        local, mesh=mesh, in_specs=placed, out_specs=P(("sp", "tp"), None), check_vma=False
    )
```

profile of v0, /device:TPU:0, one launch (start us, length us, event | category | flops | bytes accessed | tf_op | source)
XLA Modules:
  0.0 388.5 jit_solution(5894218725486632129)
XLA Ops:
  6.5 1.8 copy.47
  8.3 0.0 all-gather.5.cloned.1.call-update
  8.4 0.0 all-gather.7.cloned.1.call-start
  8.4 1.7 copy.49
  10.1 0.0 all-gather.7.cloned.1.call-update
  10.1 0.0 all-gather.9.cloned.1.call-start
  10.2 1.8 copy.51
  11.9 0.0 all-gather.9.cloned.1.call-update
  12.0 0.0 all-reduce.2.cloned.1.call-start
  12.0 0.8 copy.52
  12.8 0.1 reshape.435
  13.0 0.1 reshape.434
  13.1 1.0 copy.48
  14.1 0.1 copy.50
  14.2 0.6 slice.12
  14.8 0.5 slice.13
  15.9 22.3 %all-gather = s32[8,1,256]{2,1,0:T(1,128)S(1)} all-gather(s32[1,1,256]{2,1,0:T(1,128)S(1)} %bitcast.92), channel_id=1, replica_groups=mesh['sp'=8,'tp'=4] {'sp'}, dimensions={0}, use_global_device_ids=true | all-gather | bytes 9216 | tf_op jit(solution)/shard_map/all_gather | solution.py:94
  38.2 0.6 reduce_max.29
  40.0 2.3 reduce-window.6
  42.3 0.3 slice_reduce_fusion
  42.6 0.2 reduce-window.9
  42.8 0.1 add_bitcast_fusion
  42.9 8.6 %all-gather.5.cloned.1.call-done = bf16[2048,256]{0,1:T(8,128)(2,1)} async-done(((bf16[256,256]{0,1:T(8,128)(2,1)}), bf16[2048,256]{0,1:T(8,128)(2,1)}) %all-gather.5.cloned.1.call-update) | async-done | bytes 1048592 | tf_op jit(solution)/shard_map/all_gather | solution.py:91
  51.6 40.5 %all-gather.7.cloned.1.call-done = bf16[2048,256]{0,1:T(8,128)(2,1)} async-done(((bf16[256,256]{0,1:T(8,128)(2,1)}), bf16[2048,256]{0,1:T(8,128)(2,1)}) %all-gather.7.cloned.1.call-update) | async-done | bytes 1048592 | tf_op jit(solution)/shard_map/all_gather | solution.py:71
  92.0 12.4 %conditional.2 = (f32[4,256]{1,0:T(4,128)}, f32[4,256]{1,0:T(4,128)S(1)}, f32[4,256]{1,0:T(4,128)}, f32[4,256]{1,0:T(4,128)S(1)}) conditional(s32[]{:T(128)} %convert_element_type.53, () %tuple.24, (s32[256]{0:T(256)S(1)}, s32[2048]{0:T(1024)S(1)}, s32[256]{0:T(256)S(1)}, bf16[2048,256]{0,1:T(8,128)(2,1)}, bf16[256,4,64]{0,2,1:T(8,128)(2,1)S(1)}, ...), branch_computations={%region_1.0_spmd, %region_2.7_spmd} | conditional | flops 571996160 | bytes 50120764 | solution.py:90
  92.0 2.6 fusion.55
  94.6 0.5 fusion.2
  95.2 3.1 fusion.1
  98.3 0.6 broadcast_maximum_fusion
  98.9 5.5 %select_reduce_fusion = (f32[4,256]{1,0:T(4,128)S(1)}, f32[4,256]{1,0:T(4,128)S(1)}) fusion(f32[4,256,2048]{2,1,0:T(8,128)S(1)} %get-tuple-element.106, f32[4,256]{1,0:T(4,128)} %get-tuple-element.122, pred[256,2048]{1,0:T(8,128)(4,1)S(1)} %fusion.2, f32[4,256]{1,0:T(4,128)} %get-tuple-element.120, f32[4,256,2048]{2,1,0:T(8,128)S(1)} %fusion.55), kind=kLoop, calls=%fused_computation.2 | loop fusion | flops 20969472 | bytes 17317888 | tf_op jit(solution)/shard_map/cond/branch_1_fun/reduce_sum | solution.py:84
  104.4 39.0 %all-gather.9.cloned.1.call-done = bf16[2048,512]{0,1:T(8,128)(2,1)} async-done(((bf16[256,512]{0,1:T(8,128)(2,1)}), bf16[2048,512]{0,1:T(8,128)(2,1)}) %all-gather.9.cloned.1.call-update) | async-done | bytes 2097168 | tf_op jit(solution)/shard_map/all_gather | solution.py:93
  143.5 16.7 %conditional.3 = (f32[4,256,128]{1,2,0:T(8,128)S(1)}, f32[4,256,1]{1,0,2:T(4,128)S(1)}) conditional(s32[]{:T(128)} %convert_element_type.53, () %tuple.23, (s32[256]{0:T(256)S(1)}, s32[2048]{0:T(1024)S(1)}, s32[256]{0:T(256)S(1)}, bf16[2048,256]{0,1:T(8,128)(2,1)}, bf16[256,4,64]{0,2,1:T(8,128)(2,1)S(1)}, /*index=5*/f32[4,256]{1,0:T(4,128)}, ...), branch_computations={%region_7.8_spmd, %region_8.0_spmd} | conditional | flops 1098644480 | bytes 22837280 | solution.py:116
  143.5 5.7 %fusion.56 = f32[4,256,2048]{2,1,0:T(8,128)} fusion(bf16[256,4,64]{0,2,1:T(8,128)(2,1)S(1)} %get-tuple-element.58, bf16[2048,4,64]{0,2,1:T(8,128)(2,1)} %bitcast.75), kind=kOutput, calls=%fused_computation.113 | convolution fusion | flops 268435456 | bytes 9568256 | tf_op jit(solution)/shard_map/cond/branch_1_fun/qhd,khd->hqk/dot_general | solution.py:62
  149.2 1.4 fusion.9
  150.6 9.6 %multiply_reduce_fusion = (f32[4,256]{1,0:T(4,128)S(1)}, f32[4,256,128]{1,2,0:T(8,128)S(1)}) fusion(bf16[2048,4,128]{0,2,1:T(8,128)(2,1)} %bitcast.95, f32[4,256,2048]{2,1,0:T(8,128)} %fusion.56, bf16[256,4,64]{0,2,1:T(8,128)(2,1)S(1)} %get-tuple-element.63, bf16[2048,4,64]{0,2,1:T(8,128)(2,1)} %bitcast.82, f32[4,256]{1,0:T(4,128)S(1)} %get-tuple-element.66, ...), kind=kOutput, calls=%fused_computation.21 | convolution fusion | flops 828636160 | bytes 12734480 | tf_op jit(solution)/shard_map/cond/branch_1_fun/hqk,khv->hqv/dot_general | solution.py:109
  160.3 0.1 multiply_convert_fusion.1
  160.4 0.0 copy-start.1
  160.4 3.4 convolution_convert_fusion.1
  163.8 0.0 all-reduce.2.cloned.1.call-update
  163.9 0.3 fusion.18
  164.2 0.1 broadcast_in_dim.114
  164.3 0.3 select_reduce_fusion.2
  164.6 33.9 %all-reduce.2.cloned.1.call-done = bf16[256,2048]{1,0:T(8,128)(2,1)} async-done(((bf16[256,2048]{1,0:T(8,128)(2,1)}), bf16[256,2048]{1,0:T(8,128)(2,1)}) %all-reduce.2.cloned.1.call-update) | async-done | bytes 1048592 | tf_op jit(solution)/shard_map/psum | solution.py:124
  198.5 3.1 convert_add_fusion
  201.6 0.6 multiply_convert_fusion
  202.2 3.3 gather_fusion
  205.5 1.8 broadcast_select_fusion
  207.3 53.2 %all_to_all.10 = bf16[8,64,2048]{2,1,0:T(8,128)(2,1)S(1)} all-to-all(bf16[8,64,2048]{2,1,0:T(8,128)(2,1)S(1)} %broadcast_select_fusion), channel_id=1, replica_groups=mesh['sp'=8,'tp'=4] {'sp'}, dimensions={0} | all-to-all | bytes 4194304 | tf_op jit(solution)/shard_map/all_to_all | solution.py:148
  260.5 1.3 copy-done.4
  261.8 2.2 fusion.16
  264.1 6.3 %convolution_convert_fusion = bf16[512,2048]{1,0:T(8,128)(2,1)} fusion(bf16[1,512,2048]{2,1,0:T(8,128)(2,1)S(1)} %copy-done, bf16[512,2048]{1,0:T(8,128)(2,1)} %bitcast.78, bf16[1,2048,512]{2,1,0:T(8,128)(2,1)} %param.37, f32[512,512]{1,0:T(8,128)} %fusion.16), kind=kOutput, calls=%fused_computation.25 | convolution fusion | flops 2150105088 | bytes 9437184 | tf_op jit(solution)/shard_map/dot_general | solution.py:154
  270.3 4.5 %all-to-all-start.1 = ((bf16[8,64,2048]{2,1,0:T(8,128)(2,1)}), bf16[8,64,2048]{2,1,0:T(8,128)(2,1)}, u32[]{:S(2)}, u32[]{:S(2)}) async-start(bf16[8,64,2048]{2,1,0:T(8,128)(2,1)} %bitcast.76), calls=%async_computation.1 | async-start | bytes 4194304 | tf_op jit(solution)/shard_map/all_to_all | solution.py:157
  274.8 0.0 reduce-scatter.2.cloned.1.call-start
  274.9 0.1 reshape.440
  275.1 0.1 copy.55
  275.3 1.5 fusion.57
  276.7 45.4 %all-to-all-done.1 = bf16[8,64,2048]{2,1,0:T(8,128)(2,1)} async-done(((bf16[8,64,2048]{2,1,0:T(8,128)(2,1)}), bf16[8,64,2048]{2,1,0:T(8,128)(2,1)}, u32[]{:S(2)}, u32[]{:S(2)}) %all-to-all-start.1) | async-done | bytes 2097184 | tf_op jit(solution)/shard_map/all_to_all | solution.py:157
  322.1 10.7 %gather_fusion.1 = bf16[1024,2048]{1,0:T(8,128)(2,1)} fusion(bf16[512,2048]{1,0:T(8,128)(2,1)} %bitcast.24, s32[1024]{0:T(1024)S(1)} %broadcast_clamp_fusion), kind=kCustom, calls=%fused_computation.1 | custom fusion | bytes 8392704 | tf_op jit(solution)/shard_map/gather | solution.py:165
  332.8 8.3 %reshape.441 = f32[256,4,2048]{2,1,0:T(4,128)} reshape(bf16[1024,2048]{1,0:T(8,128)(2,1)} %gather_fusion.1) | data formatting | bytes 12582912 | tf_op jit(solution)/shard_map/convert_element_type | solution.py:165
  341.1 11.4 %multiply_reduce_fusion.1 = f32[256,2048]{1,0:T(8,128)} fusion(f32[256,4,2048]{2,1,0:T(4,128)} %reshape.441, f32[256,4]{1,0:T(8,128)S(1)} %copy.55), kind=kLoop, calls=%fused_computation.24 | loop fusion | flops 3670016 | bytes 10489856 | tf_op jit(solution)/shard_map/reduce_sum | solution.py:167
  352.5 3.7 fusion.12
  356.2 0.0 reduce-scatter.2.cloned.1.call-update
  356.2 23.9 %reduce-scatter.2.cloned.1.call-done = bf16[64,2048]{1,0:T(8,128)(2,1)} async-done(((bf16[256,2048]{1,0:T(8,128)(2,1)}), bf16[64,2048]{1,0:T(8,128)(2,1)}) %reduce-scatter.2.cloned.1.call-update) | async-done | bytes 262160 | tf_op jit(solution)/shard_map/reduce_scatter | solution.py:175
  380.1 1.9 add_convert_fusion
  (42 shorter events, 0.2 us)
Async XLA Ops:
  6.5 257.5 %copy-start = (bf16[1,512,2048]{2,1,0:T(8,128)(2,1)S(1)}, bf16[1,512,2048]{2,1,0:T(8,128)(2,1)}, u32[]{:S(2)}) copy-start(bf16[1,512,2048]{2,1,0:T(8,128)(2,1)} %param.38) | copy-start | bytes 6291460
  6.5 7.6 %copy-start.6 = (bf16[256,256]{1,0:T(8,128)(2,1)S(1)}, bf16[256,256]{1,0:T(8,128)(2,1)}, u32[]{:S(2)}) copy-start(bf16[256,256]{1,0:T(8,128)(2,1)} %param.25) | copy-start | bytes 393220
  6.5 8.3 %copy-start.8 = (s32[256]{0:T(256)S(1)}, s32[256]{0:T(256)}, u32[]{:S(2)}) copy-start(s32[256]{0:T(256)} %param.29) | copy-start | bytes 3076
  6.5 45.0 %all-gather.5.cloned.1.call-start = ((), (), s32[]{:S(2)}) async-start(), calls=%async_computation.3 | async-start | bytes 1179648 | tf_op jit(solution)/shard_map/all_gather | solution.py:91
  8.4 83.7 %all-gather.7.cloned.1.call-start = ((), (), s32[]{:S(2)}) async-start(), calls=%async_computation.4 | async-start | bytes 1179648 | tf_op jit(solution)/shard_map/all_gather | solution.py:71
  10.1 133.4 %all-gather.9.cloned.1.call-start = ((), (), s32[]{:S(2)}) async-start(), calls=%async_computation.5 | async-start | bytes 2359296 | tf_op jit(solution)/shard_map/all_gather | solution.py:93
  12.0 186.5 %all-reduce.2.cloned.1.call-start = ((), (), s32[]{:S(2)}) async-start(), calls=%async_computation.6 | async-start | bytes 2097152 | tf_op jit(solution)/shard_map/psum | solution.py:124
  92.0 51.5 %copy-start.13 = (f32[4]{0:T(128)S(1)}, f32[4]{0:T(128)}, u32[]{:S(2)}) copy-start(f32[4]{0:T(128)} %param.30) | copy-start | bytes 52
  92.0 3.2 copy-start.5
  143.5 16.8 %copy-start.11 = (f32[128]{0:T(128)S(1)}, f32[128]{0:T(128)}, u32[]{:S(2)}) copy-start(f32[128]{0:T(128)} %param.31) | copy-start | bytes 1540
  160.4 38.1 %copy-start.1 = (bf16[256,2048]{1,0:T(8,128)(2,1)S(1)}, bf16[256,2048]{1,0:T(8,128)(2,1)}, u32[]{:S(2)}) copy-start(bf16[256,2048]{1,0:T(8,128)(2,1)} %param.23) | copy-start | bytes 3145732
  164.6 37.0 %copy-start.9 = (f32[2048]{0:T(1024)S(1)}, f32[2048]{0:T(1024)}, u32[]{:S(2)}) copy-start(f32[2048]{0:T(1024)} %param.33) | copy-start | bytes 24580
  198.5 3.1 copy-start.2
  198.5 3.1 copy-start.3
  207.3 54.5 %copy-start.12 = (bf16[1,2048,512]{2,1,0:T(8,128)(2,1)S(1)}, bf16[1,2048,512]{2,1,0:T(8,128)(2,1)}, u32[]{:S(2)}) copy-start(bf16[1,2048,512]{2,1,0:T(8,128)(2,1)} %param.36) | copy-start | bytes 6291460
  260.5 1.3 copy-start.4
  270.3 4.7 %copy-start.7 = (s32[256,4]{0,1:T(4,128)S(1)}, s32[256,4]{0,1:T(4,128)}, u32[]{:S(2)}) copy-start(s32[256,4]{0,1:T(4,128)} %param.34) | copy-start | bytes 12292
  270.3 4.7 %copy-start.10 = (f32[256,4]{0,1:T(4,128)S(1)}, f32[256,4]{0,1:T(4,128)}, u32[]{:S(2)}) copy-start(f32[256,4]{0,1:T(4,128)} %param.35) | copy-start | bytes 12292
  270.3 51.7 %all-to-all-start.1 = ((bf16[8,64,2048]{2,1,0:T(8,128)(2,1)}), bf16[8,64,2048]{2,1,0:T(8,128)(2,1)}, u32[]{:S(2)}, u32[]{:S(2)}) async-start(bf16[8,64,2048]{2,1,0:T(8,128)(2,1)} %bitcast.76), calls=%async_computation.1 | async-start | bytes 4194304 | tf_op jit(solution)/shard_map/all_to_all | solution.py:157
  274.8 105.3 %reduce-scatter.2.cloned.1.call-start = ((), (), s32[]{:S(2)}) async-start(), calls=%async_computation.7 | async-start | bytes 1310720 | tf_op jit(solution)/shard_map/reduce_scatter | solution.py:175
Sparse Core Ops, SparseCore 0:
  9.4 42.1 all-gather.4
  53.6 38.3 all-gather.6
  94.1 49.3 all-gather.8
  164.0 34.4 all-reduce.1
  356.3 23.7 reduce-scatter.1
where the time goes:
time: 389 us
  waiting for transfers between devices  191 us (49%)
  blocking collectives  75.5 us (19%)
  matrix products  38.2 us (10%)
  local copies, waits for them, and re-layouts  32.8 us (8%)
  other arithmetic  30.8 us (8%)
  between operations  15.1 us (4%)
  starting transfers between devices  4.67 us (1%)
    all_to_all x1, blocking collectives, local(): lax.all_to_all(outgoing, 'sp', split_axis=0, concat_axis=0, tiled=True)  53.2 us
    all_to_all x1, waiting for transfers between devices, local(): lax.all_to_all(result.reshape(seq_size, item_count, model_width), 'sp', s...  45.4 us
    all_gather x1, waiting for transfers between devices, local(): key_second = lax.all_gather(key_two, 'sp', axis=0, tiled=True)  40.5 us
    all_gather x1, waiting for transfers between devices, local(): value_block = lax.all_gather(values, 'sp', axis=0, tiled=True)  39 us
    psum x1, waiting for transfers between devices, local(): lax.psum(proj_term.astype(jnp.bfloat16), 'tp').astype(jnp.float32)  33.9 us
    reduce_scatter x1, waiting for transfers between devices, local(): lax.psum_scatter((routed + shared_out).astype(jnp.bfloat16), 'tp', scatte...  23.9 us
    all_gather x1, blocking collectives, local(): apply_key_docs = lax.all_gather(documents, 'sp', axis=0, tiled=True)  22.3 us
    dot_general x3, matrix products, scores(): jnp.einsum('qhd,khd->hqk', query_block, keyed, preferred_element_type=jnp...  11.5 us
  transfers between devices with their start and end apart: 6, of which 6 were waited for; matrix products, arithmetic and copies ran while one was open for 6% of the time, Pallas kernels for 0%

commit v1 on v0

--- a/solution.py
+++ b/solution.py
@@ -121,7 +121,9 @@
     share_rows = tok_rows // tp_size
     own_start = lax.axis_index("tp") * share_rows
     proj_term = jnp.dot(attn_rows, out_weight, preferred_element_type=jnp.float32)
-    projected = lax.psum(proj_term.astype(jnp.bfloat16), "tp").astype(jnp.float32)
+    projected = jnp.sum(lax.all_gather(proj_term.astype(jnp.bfloat16), "tp"), axis=0).astype(
+        jnp.float32
+    )
     mixed_all = resid.astype(jnp.float32) + projected
     normed_all = (mixed_all * rms_scale(mixed_all, 1e-06) * ffn_gain).astype(jnp.bfloat16)
     mixed_own = lax.dynamic_slice_in_dim(mixed_all, own_start, share_rows, 0)

time: 389 us -> 391 us (level)
    psum x1 -> x0, waiting for transfers between devices: 33.9 us -> none  [local(): lax.psum(proj_term.astype(jnp.bfloat16), 'tp').astype(jnp.float32)]
    all_gather x0 -> x1, waiting for transfers between devices: none -> 28.8 us  [local(): lax.all_gather(proj_term.astype(jnp.bfloat16), 'tp')]
    unnamed x32 -> x28, local copies, waits for them, and re-layouts: 8.52 us -> 8.75 us
where the time goes in v1:
time: 391 us; the launch traced here: 390 us
  waiting for transfers between devices  189 us (48%)
  blocking collectives  76.3 us (20%)
  matrix products  37.9 us (10%)
  other arithmetic  34.4 us (9%)
  local copies, waits for them, and re-layouts  33.1 us (8%)
  between operations  15.1 us (4%)
  starting transfers between devices  4.67 us (1%)
    all_to_all x1, blocking collectives, local(): lax.all_to_all(outgoing, 'sp', split_axis=0, concat_axis=0, tiled=True)  54 us
    all_to_all x1, waiting for transfers between devices, local(): lax.all_to_all(result.reshape(seq_size, item_count, model_width), 'sp', s...  45.7 us
    all_gather x1, waiting for transfers between devices, local(): key_second = lax.all_gather(key_two, 'sp', axis=0, tiled=True)  40.5 us
    all_gather x1, waiting for transfers between devices, local(): value_block = lax.all_gather(values, 'sp', axis=0, tiled=True)  39 us
    all_gather x1, waiting for transfers between devices, local(): lax.all_gather(proj_term.astype(jnp.bfloat16), 'tp')  28.8 us
    reduce_scatter x1, waiting for transfers between devices, local(): lax.psum_scatter((routed + shared_out).astype(jnp.bfloat16), 'tp', scatte...  23 us
    all_gather x1, blocking collectives, local(): apply_key_docs = lax.all_gather(documents, 'sp', axis=0, tiled=True)  22.3 us
    all_gather x1, waiting for transfers between devices, local(): apply_key_first = lax.all_gather(key_one, 'sp', axis=0, tiled=True)  11.7 us
  transfers between devices with their start and end apart: 6, of which 6 were waited for; matrix products, arithmetic and copies ran while one was open for 6% of the time, Pallas kernels for 0%

profile of v1, /device:TPU:0, one launch (start us, length us, event | category | flops | bytes accessed | tf_op | source)
XLA Modules:
  0.0 390.4 jit_solution(16356775428166009943)
XLA Ops:
  6.5 1.8 copy.47
  8.3 0.0 all-gather.7.cloned.1.call-update
  8.4 0.0 all-gather.9.cloned.1.call-start
  8.4 1.7 copy.49
  10.1 0.0 all-gather.9.cloned.1.call-update
  10.1 0.0 all-gather.11.cloned.1.call-start
  10.2 1.8 copy.51
  12.0 0.0 all-gather.11.cloned.1.call-update
  12.0 0.0 all-gather.13.cloned.1.call-start
  12.0 1.0 copy.48
  13.0 1.0 copy.50
  14.1 0.6 slice.12
  14.6 0.5 slice.13
  15.7 22.3 %all-gather.1 = s32[8,1,256]{2,1,0:T(1,128)S(1)} all-gather(s32[1,1,256]{2,1,0:T(1,128)S(1)} %bitcast.94), channel_id=1, replica_groups=mesh['sp'=8,'tp'=4] {'sp'}, dimensions={0}, use_global_device_ids=true | all-gather | bytes 9216 | tf_op jit(solution)/shard_map/all_gather | solution.py:94
  38.0 0.6 reduce_max.29
  39.8 11.7 %all-gather.7.cloned.1.call-done = bf16[2048,256]{0,1:T(8,128)(2,1)} async-done(((bf16[256,256]{0,1:T(8,128)(2,1)}), bf16[2048,256]{0,1:T(8,128)(2,1)}) %all-gather.7.cloned.1.call-update) | async-done | bytes 1048592 | tf_op jit(solution)/shard_map/all_gather | solution.py:91
  51.5 40.5 %all-gather.9.cloned.1.call-done = bf16[2048,256]{0,1:T(8,128)(2,1)} async-done(((bf16[256,256]{0,1:T(8,128)(2,1)}), bf16[2048,256]{0,1:T(8,128)(2,1)}) %all-gather.9.cloned.1.call-update) | async-done | bytes 1048592 | tf_op jit(solution)/shard_map/all_gather | solution.py:71
  92.0 12.4 %conditional.2 = (f32[4,256]{1,0:T(4,128)}, f32[4,256]{1,0:T(4,128)S(1)}, f32[4,256]{1,0:T(4,128)}, f32[4,256]{1,0:T(4,128)S(1)}) conditional(s32[]{:T(128)} %convert_element_type.55, () %tuple.24, (s32[256]{0:T(256)S(1)}, s32[2048]{0:T(1024)S(1)}, s32[256]{0:T(256)S(1)}, bf16[2048,256]{0,1:T(8,128)(2,1)}, bf16[256,4,64]{0,2,1:T(8,128)(2,1)S(1)}, ...), branch_computations={%region_1.0_spmd, %region_2.7_spmd} | conditional | flops 571996160 | bytes 50120764 | solution.py:90
  92.0 2.6 fusion.55
  94.6 0.5 fusion.2
  95.2 3.1 fusion.1
  98.3 0.6 broadcast_maximum_fusion
  98.9 5.5 %select_reduce_fusion = (f32[4,256]{1,0:T(4,128)S(1)}, f32[4,256]{1,0:T(4,128)S(1)}) fusion(f32[4,256,2048]{2,1,0:T(8,128)S(1)} %get-tuple-element.106, f32[4,256]{1,0:T(4,128)} %get-tuple-element.122, pred[256,2048]{1,0:T(8,128)(4,1)S(1)} %fusion.2, f32[4,256]{1,0:T(4,128)} %get-tuple-element.120, f32[4,256,2048]{2,1,0:T(8,128)S(1)} %fusion.55), kind=kLoop, calls=%fused_computation.2 | loop fusion | flops 20969472 | bytes 17317888 | tf_op jit(solution)/shard_map/cond/branch_1_fun/reduce_sum | solution.py:84
  104.5 39.0 %all-gather.11.cloned.1.call-done = bf16[2048,512]{0,1:T(8,128)(2,1)} async-done(((bf16[256,512]{0,1:T(8,128)(2,1)}), bf16[2048,512]{0,1:T(8,128)(2,1)}) %all-gather.11.cloned.1.call-update) | async-done | bytes 2097168 | tf_op jit(solution)/shard_map/all_gather | solution.py:93
  143.5 15.8 %conditional.3 = (f32[4,256,128]{1,2,0:T(8,128)S(1)}, f32[4,256,1]{1,0,2:T(4,128)S(1)}) conditional(s32[]{:T(128)} %convert_element_type.55, () %tuple.23, (s32[256]{0:T(256)S(1)}, s32[2048]{0:T(1024)S(1)}, s32[256]{0:T(256)S(1)}, bf16[2048,256]{0,1:T(8,128)(2,1)}, bf16[256,4,64]{0,2,1:T(8,128)(2,1)S(1)}, /*index=5*/f32[4,256]{1,0:T(4,128)}, ...), branch_computations={%region_7.8_spmd, %region_8.0_spmd} | conditional | flops 1098644480 | bytes 22837280 | solution.py:116
  143.5 5.7 %fusion.56 = f32[4,256,2048]{2,1,0:T(8,128)} fusion(bf16[256,4,64]{0,2,1:T(8,128)(2,1)S(1)} %get-tuple-element.58, bf16[2048,4,64]{0,2,1:T(8,128)(2,1)} %bitcast.76), kind=kOutput, calls=%fused_computation.113 | convolution fusion | flops 268435456 | bytes 9568256 | tf_op jit(solution)/shard_map/cond/branch_1_fun/qhd,khd->hqk/dot_general | solution.py:62
  149.2 0.5 fusion.9
  149.8 9.5 %multiply_reduce_fusion = (f32[4,256]{1,0:T(4,128)S(1)}, f32[4,256,128]{1,2,0:T(8,128)S(1)}) fusion(bf16[2048,4,128]{0,2,1:T(8,128)(2,1)} %bitcast.97, f32[4,256,2048]{2,1,0:T(8,128)} %fusion.56, bf16[256,4,64]{0,2,1:T(8,128)(2,1)S(1)} %get-tuple-element.63, bf16[2048,4,64]{0,2,1:T(8,128)(2,1)} %bitcast.84, f32[4,256]{1,0:T(4,128)S(1)} %get-tuple-element.66, ...), kind=kOutput, calls=%fused_computation.21 | convolution fusion | flops 828636160 | bytes 12734480 | tf_op jit(solution)/shard_map/cond/branch_1_fun/hqk,khv->hqv/dot_general | solution.py:109
  159.3 0.1 multiply_convert_fusion.1
  159.4 3.3 convolution_convert_fusion.1
  162.7 0.0 all-gather.13.cloned.1.call-update
  162.8 0.1 copy.52
  162.9 0.1 reshape.435
  163.0 0.1 reshape.434
  163.2 2.3 reduce-window.6
  165.5 0.3 slice_reduce_fusion
  165.8 0.2 reduce-window.9
  166.0 0.1 add_bitcast_fusion
  166.1 0.3 fusion.18
  166.4 0.1 broadcast_in_dim.114
  166.5 0.3 select_reduce_fusion.2
  166.8 28.8 %all-gather.13.cloned.1.call-done = bf16[1024,2048]{1,0:T(8,128)(2,1)} async-done(((bf16[256,2048]{1,0:T(8,128)(2,1)}), bf16[1024,2048]{1,0:T(8,128)(2,1)}) %all-gather.13.cloned.1.call-update) | async-done | bytes 4194320 | tf_op jit(solution)/shard_map/all_gather | solution.py:124
  195.6 3.1 reduce_sum.83
  198.7 3.3 convert_add_fusion
  202.0 1.7 multiply_convert_fusion
  203.7 3.3 gather_fusion
  207.1 1.8 broadcast_select_fusion
  208.9 54.0 %all_to_all.10 = bf16[8,64,2048]{2,1,0:T(8,128)(2,1)S(1)} all-to-all(bf16[8,64,2048]{2,1,0:T(8,128)(2,1)S(1)} %broadcast_select_fusion), channel_id=1, replica_groups=mesh['sp'=8,'tp'=4] {'sp'}, dimensions={0} | all-to-all | bytes 4194304 | tf_op jit(solution)/shard_map/all_to_all | solution.py:150
  262.9 1.3 copy-done.3
  264.2 2.2 fusion.16
  266.5 6.3 %convolution_convert_fusion = bf16[512,2048]{1,0:T(8,128)(2,1)} fusion(bf16[1,512,2048]{2,1,0:T(8,128)(2,1)S(1)} %copy-done, bf16[512,2048]{1,0:T(8,128)(2,1)} %bitcast.80, bf16[1,2048,512]{2,1,0:T(8,128)(2,1)} %param.37, f32[512,512]{1,0:T(8,128)} %fusion.16), kind=kOutput, calls=%fused_computation.25 | convolution fusion | flops 2150105088 | bytes 9437184 | tf_op jit(solution)/shard_map/dot_general | solution.py:156
  272.7 4.5 %all-to-all-start.1 = ((bf16[8,64,2048]{2,1,0:T(8,128)(2,1)}), bf16[8,64,2048]{2,1,0:T(8,128)(2,1)}, u32[]{:S(2)}, u32[]{:S(2)}) async-start(bf16[8,64,2048]{2,1,0:T(8,128)(2,1)} %bitcast.78), calls=%async_computation.1 | async-start | bytes 4194304 | tf_op jit(solution)/shard_map/all_to_all | solution.py:159
  277.3 0.0 reduce-scatter.2.cloned.1.call-start
  277.3 0.1 reshape.440
  277.5 0.1 copy.55
  277.7 1.5 fusion.57
  279.1 45.7 %all-to-all-done.1 = bf16[8,64,2048]{2,1,0:T(8,128)(2,1)} async-done(((bf16[8,64,2048]{2,1,0:T(8,128)(2,1)}), bf16[8,64,2048]{2,1,0:T(8,128)(2,1)}, u32[]{:S(2)}, u32[]{:S(2)}) %all-to-all-start.1) | async-done | bytes 2097184 | tf_op jit(solution)/shard_map/all_to_all | solution.py:159
  324.8 10.7 %gather_fusion.1 = bf16[1024,2048]{1,0:T(8,128)(2,1)} fusion(bf16[512,2048]{1,0:T(8,128)(2,1)} %bitcast.25, s32[1024]{0:T(1024)S(1)} %broadcast_clamp_fusion), kind=kCustom, calls=%fused_computation.1 | custom fusion | bytes 8392704 | tf_op jit(solution)/shard_map/gather | solution.py:167
  335.5 8.3 %reshape.441 = f32[256,4,2048]{2,1,0:T(4,128)} reshape(bf16[1024,2048]{1,0:T(8,128)(2,1)} %gather_fusion.1) | data formatting | bytes 12582912 | tf_op jit(solution)/shard_map/convert_element_type | solution.py:167
  343.8 11.4 %multiply_reduce_fusion.1 = f32[256,2048]{1,0:T(8,128)} fusion(f32[256,4,2048]{2,1,0:T(4,128)} %reshape.441, f32[256,4]{1,0:T(8,128)S(1)} %copy.55), kind=kLoop, calls=%fused_computation.24 | loop fusion | flops 3670016 | bytes 10489856 | tf_op jit(solution)/shard_map/reduce_sum | solution.py:169
  355.2 3.7 fusion.12
  358.9 0.0 reduce-scatter.2.cloned.1.call-update
  358.9 23.0 %reduce-scatter.2.cloned.1.call-done = bf16[64,2048]{1,0:T(8,128)(2,1)} async-done(((bf16[256,2048]{1,0:T(8,128)(2,1)}), bf16[64,2048]{1,0:T(8,128)(2,1)}) %reduce-scatter.2.cloned.1.call-update) | async-done | bytes 262160 | tf_op jit(solution)/shard_map/reduce_scatter | solution.py:177
  382.0 1.9 add_convert_fusion
  (39 shorter events, 0.2 us)
Async XLA Ops:
  6.5 259.9 %copy-start = (bf16[1,512,2048]{2,1,0:T(8,128)(2,1)S(1)}, bf16[1,512,2048]{2,1,0:T(8,128)(2,1)}, u32[]{:S(2)}) copy-start(bf16[1,512,2048]{2,1,0:T(8,128)(2,1)} %param.38) | copy-start | bytes 6291460
  6.5 8.1 %copy-start.6 = (s32[256]{0:T(256)S(1)}, s32[256]{0:T(256)}, u32[]{:S(2)}) copy-start(s32[256]{0:T(256)} %param.29) | copy-start | bytes 3076
  6.5 45.0 %all-gather.7.cloned.1.call-start = ((), (), s32[]{:S(2)}) async-start(), calls=%async_computation.3 | async-start | bytes 1179648 | tf_op jit(solution)/shard_map/all_gather | solution.py:91
  8.4 83.7 %all-gather.9.cloned.1.call-start = ((), (), s32[]{:S(2)}) async-start(), calls=%async_computation.4 | async-start | bytes 1179648 | tf_op jit(solution)/shard_map/all_gather | solution.py:71
  10.1 133.4 %all-gather.11.cloned.1.call-start = ((), (), s32[]{:S(2)}) async-start(), calls=%async_computation.5 | async-start | bytes 2359296 | tf_op jit(solution)/shard_map/all_gather | solution.py:93
  12.0 183.6 %all-gather.13.cloned.1.call-start = ((), (), s32[]{:S(2)}) async-start(), calls=%async_computation.7 | async-start | bytes 5242880 | tf_op jit(solution)/shard_map/all_gather | solution.py:124
  92.0 51.5 %copy-start.11 = (f32[4]{0:T(128)S(1)}, f32[4]{0:T(128)}, u32[]{:S(2)}) copy-start(f32[4]{0:T(128)} %param.30) | copy-start | bytes 52
  92.0 3.2 copy-start.4
  143.5 15.8 %copy-start.9 = (f32[128]{0:T(128)S(1)}, f32[128]{0:T(128)}, u32[]{:S(2)}) copy-start(f32[128]{0:T(128)} %param.31) | copy-start | bytes 1540
  159.4 3.3 copy-start.5
  198.6 3.4 copy-start.1
  198.7 3.3 copy-start.2
  198.7 3.3 copy-start.7
  208.9 55.4 %copy-start.10 = (bf16[1,2048,512]{2,1,0:T(8,128)(2,1)S(1)}, bf16[1,2048,512]{2,1,0:T(8,128)(2,1)}, u32[]{:S(2)}) copy-start(bf16[1,2048,512]{2,1,0:T(8,128)(2,1)} %param.36) | copy-start | bytes 6291460
  262.9 1.3 copy-start.3
  272.7 4.7 %copy-start.8 = (f32[256,4]{0,1:T(4,128)S(1)}, f32[256,4]{0,1:T(4,128)}, u32[]{:S(2)}) copy-start(f32[256,4]{0,1:T(4,128)} %param.35) | copy-start | bytes 12292
  272.7 52.1 %all-to-all-start.1 = ((bf16[8,64,2048]{2,1,0:T(8,128)(2,1)}), bf16[8,64,2048]{2,1,0:T(8,128)(2,1)}, u32[]{:S(2)}, u32[]{:S(2)}) async-start(bf16[8,64,2048]{2,1,0:T(8,128)(2,1)} %bitcast.78), calls=%async_computation.1 | async-start | bytes 4194304 | tf_op jit(solution)/shard_map/all_to_all | solution.py:159
  277.3 104.7 %reduce-scatter.2.cloned.1.call-start = ((), (), s32[]{:S(2)}) async-start(), calls=%async_computation.6 | async-start | bytes 1310720 | tf_op jit(solution)/shard_map/reduce_scatter | solution.py:177
Sparse Core Ops, SparseCore 0:
  9.4 42.1 all-gather.6
  53.6 38.3 all-gather.8
  94.1 49.3 all-gather.10
  162.9 32.6 all-gather.12
  359.1 22.8 reduce-scatter.1
